TPU v7x, 32 devices: a whole 2x2x4 slice. The times are simulated.
32 devices in a mesh: sp: 4 (over y, core), tp: 8 (over z, x).
Axes of the slice: x: 2, y: 2, z: 4, core: 2. Of those that a mesh axis runs over, the one named last changes fastest.
Arguments:
- latent: bfloat16 [960, 2048], P(('sp', 'tp')), may hold values from -40 to 40
- context: bfloat16 [768, 2048], P('sp'), may hold values from -6 to 6
- cond_latent: float32 [2048], P('sp'), may hold values from -6 to 6
- cond_context: float32 [2048], P('sp'), may hold values from -6 to 6
- mod_weight: bfloat16 [2048, 6144], P('sp', 'tp'), may hold values from -0.125 to 0.125
- w_query: bfloat16 [2048, 1024], P(None, 'tp'), may hold values from -5 to 5
- w_key: bfloat16 [2048, 1024], P(None, 'tp'), may hold values from -5 to 5
- w_value: bfloat16 [2048, 1024], P(None, 'tp'), may hold values from -0.125 to 0.125
- w_out: bfloat16 [1024, 2048], P('tp'), may hold values from -0.1875 to 0.1875
- head_lambda: float32 [8], P('tp'), may hold values from 0.3 to 0.8
Outputs:
- mixed_latent: bfloat16 [960, 2048], P(('sp', 'tp'))
All inputs are finite; a program needn't handle non-finite values.
Results may differ from a plain program's by a relative error of at most 0.011.
Values may be sent and summed in bfloat16 or wider, within the bound.
A program may use at most 64 MiB of HBM per device.

v0:
```python
import jax
import jax.numpy as jnp
from jax import lax
from jax.sharding import PartitionSpec as P

QK_DIM = 64
VAL_DIM = 128
GRID_W = 64
NORM_EPS = 0.01
HEAD_EPS = 0.001
THETA = 10000.0


def modulate_rows(rows, shift, scale):
    values = rows.astype(jnp.float32)
    normed = values * lax.rsqrt(jnp.mean(values * values, axis=-1, keepdims=True) + NORM_EPS)
    return (normed * (1.0 + scale) + shift).astype(jnp.bfloat16)


def rotary_tables(positions):
    quarter = QK_DIM // 4
    inverse = THETA ** (-jnp.arange(quarter, dtype=jnp.float32) / quarter)
    grid_row = (positions // GRID_W).astype(jnp.float32)
    grid_column = (positions % GRID_W).astype(jnp.float32)
    by_row = grid_row[:, None] * inverse[None, :]
    by_column = grid_column[:, None] * inverse[None, :]
    angle = jnp.concatenate([by_row, by_row, by_column, by_column], axis=-1)
    return (jnp.cos(angle), jnp.sin(angle))


def rotate(product, cosine, sine):
    number = product.shape[0]
    quarter = QK_DIM // 4
    half = QK_DIM // 2
    shaped = product.reshape(number, -1, QK_DIM)
    first = shaped[..., :half]
    second = shaped[..., half:]
    turned = jnp.concatenate(
        [
            -first[..., quarter:],
            first[..., :quarter],
            -second[..., quarter:],
            second[..., :quarter],
        ],
        axis=-1,
    )
    result = shaped * cosine[:, None, :] + turned * sine[:, None, :]
    return result.reshape(number, -1).astype(jnp.bfloat16)


def attend_piece(state, piece, queries):
    highest, totals, carried = state
    keys, values = piece
    number = keys.shape[0]
    heads = queries.shape[1]
    key_heads = keys.reshape(number, heads, 2, QK_DIM)
    value_heads = values.reshape(number, heads, VAL_DIM)
    scores = jnp.einsum(
        "qhmd,khmd->hmqk", queries, key_heads, preferred_element_type=jnp.float32
    ) * QK_DIM ** (-0.5)
    new_highest = jnp.maximum(highest, jnp.max(scores, axis=-1))
    weights = jnp.exp(scores - new_highest[..., None])
    totals = jnp.sum(weights, axis=-1)
    mixed = jnp.einsum(
        "hmqk,khd->hmqd",
        weights.astype(jnp.bfloat16),
        value_heads,
        preferred_element_type=jnp.float32,
    )
    carried = mixed
    return (new_highest, totals, carried)


def shards(
    latent,
    context,
    cond_latent,
    cond_context,
    mod_weight,
    w_query,
    w_key,
    w_value,
    w_out,
    head_lambda,
):
    width = latent.shape[1]
    heads = head_lambda.shape[0]
    conditioned = jax.nn.silu(jnp.stack([cond_latent, cond_context])).astype(jnp.bfloat16)
    partial_mod = jnp.dot(conditioned, mod_weight, preferred_element_type=jnp.float32)
    summed = lax.psum(partial_mod, "sp")
    modulation = lax.all_gather(summed, "tp", axis=1, tiled=True)
    shift_context = modulation[1, :width]
    scale_context = modulation[1, width : 2 * width]
    gate_latent = modulation[0, 2 * width :]
    own_rows = modulate_rows(latent, modulation[0, :width], modulation[0, width : 2 * width])
    group_rows = latent.shape[0] * lax.axis_size("tp")
    offset = lax.axis_index("sp") * group_rows
    piece = lax.all_gather(own_rows, "tp", axis=0, tiled=True)
    positions = offset + jnp.arange(piece.shape[0], dtype=jnp.int32)
    cosine, sine = rotary_tables(positions)
    query_part = rotate(jnp.dot(piece, w_query, preferred_element_type=jnp.float32), cosine, sine)
    key_part = rotate(jnp.dot(piece, w_key, preferred_element_type=jnp.float32), cosine, sine)
    value_part = jnp.dot(piece, w_value, preferred_element_type=jnp.float32).astype(jnp.bfloat16)
    projected = jnp.concatenate([query_part, key_part, value_part], axis=1)
    key_columns = heads * 2 * QK_DIM
    queries = projected[:, :key_columns].reshape(group_rows, heads, 2, QK_DIM)
    keys = projected[:, key_columns : 2 * key_columns]
    values = projected[:, 2 * key_columns :]
    initial = (
        jnp.full((heads, 2, group_rows), -1e30, jnp.float32),
        jnp.zeros((heads, 2, group_rows), jnp.float32),
        jnp.zeros((heads, 2, group_rows, VAL_DIM), jnp.float32),
    )
    own_context = modulate_rows(context, shift_context, scale_context)
    context_keys = jnp.dot(own_context, w_key, preferred_element_type=jnp.float32).astype(
        jnp.bfloat16
    )
    context_values = jnp.dot(own_context, w_value, preferred_element_type=jnp.float32).astype(
        jnp.bfloat16
    )
    joined_keys = jnp.concatenate([keys, context_keys], axis=0)
    joined_values = jnp.concatenate([values, context_values], axis=0)
    state = attend_piece(
        initial,
        (
            lax.all_gather(joined_keys, "sp", axis=0, tiled=True),
            lax.all_gather(joined_values, "sp", axis=0, tiled=True),
        ),
        queries,
    )
    highest, totals, carried = state
    factor = head_lambda[:, None, None]
    head_out = (
        carried[:, 0] / totals[:, 0][..., None] - factor * carried[:, 1] / totals[:, 1][..., None]
    )
    head_out = head_out * lax.rsqrt(
        jnp.mean(head_out * head_out, axis=-1, keepdims=True) + HEAD_EPS
    )
    attended = (
        jnp.transpose(head_out, (1, 0, 2)).reshape(group_rows, heads * VAL_DIM).astype(jnp.bfloat16)
    )
    branch = lax.psum_scatter(
        jnp.dot(attended, w_out, preferred_element_type=jnp.float32),
        "tp",
        scatter_dimension=0,
        tiled=True,
    )
    branch = branch * lax.rsqrt(jnp.mean(branch * branch, axis=-1, keepdims=True) + NORM_EPS)
    return (latent.astype(jnp.float32) + gate_latent * branch).astype(jnp.bfloat16)


def solution(mesh):
    placed = (
        P(("sp", "tp"), None),
        P("sp", None),
        P("sp"),
        P("sp"),
        P("sp", "tp"),
        P(None, "tp"),
        P(None, "tp"),
        P(None, "tp"),
        P("tp", None),
        P("tp"),
    )
    return jax.shard_map(
        shards, mesh=mesh, in_specs=placed, out_specs=P(("sp", "tp"), None), check_vma=False
    )
```

profile of v0, /device:TPU:8, one launch (start us, length us, event | category | flops | bytes accessed | tf_op | source)
XLA Modules:
  0.0 153.3 jit_solution(12564381263375404381)
XLA Ops:
  0.0 1.1 fusion.14
  1.2 1.5 fusion.6
  2.7 0.9 fusion.37
  3.6 7.0 %psum.7 = f32[2,768]{1,0:T(2,128)S(1)} all-reduce(f32[2,768]{1,0:T(2,128)S(1)} %fusion.37), channel_id=1, replica_groups=mesh['sp'=4,'tp'=8] {'sp'}, use_global_device_ids=true, to_apply=%region_0.1 | all-reduce | flops 1536 | bytes 12288 | tf_op jit(solution)/shard_map/psum | solution.py:90
  10.6 28.2 %all_gather.12 = f32[2,6144]{1,0:T(2,128)S(1)} all-gather(f32[2,768]{1,0:T(2,128)S(1)} %psum.7), channel_id=1, replica_groups=mesh['sp'=4,'tp'=8] {'tp'}, dimensions={1}, use_global_device_ids=true | all-gather | bytes 55296 | tf_op jit(solution)/shard_map/all_gather | solution.py:91
  38.9 1.8 %convolution_convert_fusion.1 = bf16[192,128]{1,0:T(8,128)(2,1)S(1)} fusion(bf16[2048,128]{1,0:T(8,128)(2,1)} %param.17, bf16[192,2048]{1,0:T(8,128)(2,1)} %param.11, f32[2048]{0:T(1024)S(1)} %bitcast.84, f32[2048]{0:T(1024)S(1)} %bitcast.86, f32[192]{0:T(256)S(1)} %add_rsqrt_fusion.1), kind=kOutput, calls=%fused_computation.14 | convolution fusion | flops 102653952 | bytes 1377024 | tf_op jit(solution)/shard_map/dot_general | solution.py:118
  40.7 0.5 convolution_convert_fusion.2
  41.3 33.0 %all-gather = bf16[8,30,2048]{2,1,0:T(8,128)(2,1)S(1)} all-gather(bf16[1,30,2048]{2,1,0:T(8,128)(2,1)S(1)} %fusion.19), channel_id=1, replica_groups=mesh['sp'=4,'tp'=8] {'tp'}, dimensions={0}, use_global_device_ids=true | all-gather | bytes 1105920 | tf_op jit(solution)/shard_map/all_gather | solution.py:98
  74.3 0.3 reshape.355
  74.6 1.5 convolution_convert_fusion
  76.1 1.4 fusion.49
  78.5 0.4 fusion.48
  79.6 6.3 %all_gather.14 = bf16[1728,128]{1,0:T(8,128)(2,1)S(1)} all-gather(bf16[432,128]{1,0:T(8,128)(2,1)S(1)} %pad_maximum_fusion), channel_id=1, replica_groups=mesh['sp'=4,'tp'=8] {'sp'}, dimensions={0}, use_global_device_ids=true | all-gather | bytes 552960 | tf_op jit(solution)/shard_map/all_gather | solution.py:126
  86.1 6.8 %all_gather.15 = bf16[1728,128]{1,0:T(8,128)(2,1)S(1)} all-gather(bf16[432,128]{1,0:T(8,128)(2,1)S(1)} %pad_maximum_fusion.1), channel_id=1, replica_groups=mesh['sp'=4,'tp'=8] {'sp'}, dimensions={0}, use_global_device_ids=true | all-gather | bytes 552960 | tf_op jit(solution)/shard_map/all_gather | solution.py:127
  92.9 0.7 fusion.47
  93.7 0.6 fusion.1
  94.3 0.7 fusion.10
  95.3 0.5 fusion.28
  95.8 48.5 %fusion = f32[32,2048]{1,0:T(8,128)S(1)} fusion(f32[240,2048]{1,0:T(8,128)S(1)} %fusion.28), kind=kCustom, calls=%all-reduce-scatter | all-reduce-scatter fusion | flops 524289 | bytes 2228736
  144.3 4.3 %collective-permute-start = (f32[14,2048]{1,0:T(8,128)S(1)}, f32[14,2048]{1,0:T(8,128)S(1)}, u32[]{:S(2)}, u32[]{:S(2)}) collective-permute-start(f32[14,2048]{1,0:T(8,128)S(1)} %slice.97), channel_id=1, source_target_pairs={{0,1},{1,2},{2,3},{3,4},{4,5},{5,6},{6,7},{8,9},{9,10},{10,11},{11... | collective-permute-start | bytes 344072
  148.6 0.6 dynamic-slice.4
  149.9 2.2 %collective-permute-done = f32[14,2048]{1,0:T(8,128)S(1)} collective-permute-done((f32[14,2048]{1,0:T(8,128)S(1)}, f32[14,2048]{1,0:T(8,128)S(1)}, u32[]{:S(2)}, u32[]{:S(2)}) %collective-permute-start) | collective-permute-done | bytes 114720
  152.1 0.2 concatenate.28
  152.5 0.8 fusion.18
  (42 shorter events, 1.9 us)
Async XLA Ops:
  0.0 2.6 %copy-start = (bf16[512,768]{1,0:T(8,128)(2,1)S(1)}, bf16[512,768]{1,0:T(8,128)(2,1)}, u32[]{:S(2)}) copy-start(bf16[512,768]{1,0:T(8,128)(2,1)} %param.14) | copy-start | bytes 2359300
  1.1 39.6 %copy-start.2 = (bf16[192,2048]{1,0:T(8,128)(2,1)S(1)}, bf16[192,2048]{1,0:T(8,128)(2,1)}, u32[]{:S(2)}) copy-start(bf16[192,2048]{1,0:T(8,128)(2,1)} %param.11) | copy-start | bytes 2359300
  1.2 39.5 %copy-start.3 = (bf16[2048,128]{1,0:T(8,128)(2,1)S(1)}, bf16[2048,128]{1,0:T(8,128)(2,1)}, u32[]{:S(2)}) copy-start(bf16[2048,128]{1,0:T(8,128)(2,1)} %param.16) | copy-start | bytes 1572868
  38.9 2.3 %copy-start.1 = (bf16[30,2048]{1,0:T(8,128)(2,1)S(1)}, bf16[30,2048]{1,0:T(8,128)(2,1)}, u32[]{:S(2)}) copy-start(bf16[30,2048]{1,0:T(8,128)(2,1)} %param.10) | copy-start | bytes 368644
  74.6 4.0 %copy-start.4 = (bf16[2048,128]{1,0:T(8,128)(2,1)S(1)}, bf16[2048,128]{1,0:T(8,128)(2,1)}, u32[]{:S(2)}) copy-start(bf16[2048,128]{1,0:T(8,128)(2,1)} %param.15) | copy-start | bytes 1572868
  94.3 1.0 copy-start.5
  95.3 53.3 %copy-start.6 = (u32[32]{0:T(128)S(1)}, u32[32]{0:T(128)}, u32[]{:S(2)}) copy-start(u32[32]{0:T(128)} %constant.70) | copy-start | bytes 388
  144.3 7.8 %collective-permute-start = (f32[14,2048]{1,0:T(8,128)S(1)}, f32[14,2048]{1,0:T(8,128)S(1)}, u32[]{:S(2)}, u32[]{:S(2)}) collective-permute-start(f32[14,2048]{1,0:T(8,128)S(1)} %slice.97), channel_id=1, source_target_pairs={{0,1},{1,2},{2,3},{3,4},{4,5},{5,6},{6,7},{8,9},{9,10},{10,11},{11... | collective-permute-start | bytes 344072
where the time goes:
time: 154 us; the launch traced here: 153 us
  blocking collectives  130 us (84%)
  matrix products  8.4 us (5%)
  other arithmetic  4.88 us (3%)
  starting transfers between devices  4.27 us (3%)
  waiting for transfers between devices  2.24 us (1%)
  local copies, waits for them, and re-layouts  2.05 us (1%)
  between operations  1.61 us (1%)
    unnamed x1, blocking collectives  48.5 us
    all_gather x1, blocking collectives, shards(): piece = lax.all_gather(own_rows, 'tp', axis=0, tiled=True)  33 us
    all_gather x1, blocking collectives, shards(): modulation = lax.all_gather(summed, 'tp', axis=1, tiled=True)  28.2 us
    psum x1, blocking collectives, shards(): summed = lax.psum(partial_mod, 'sp')  7.04 us
    all_gather x1, blocking collectives, shards(): lax.all_gather(joined_values, 'sp', axis=0, tiled=True)  6.83 us
    all_gather x1, blocking collectives, shards(): lax.all_gather(joined_keys, 'sp', axis=0, tiled=True)  6.28 us
    unnamed x1, starting transfers between devices  4.27 us
  transfers between devices with their start and end apart: 1, of which 1 were waited for; matrix products, arithmetic and copies ran while one was open for 0% of the time, Pallas kernels for 0%

commit v1 on v0

--- a/solution.py
+++ b/solution.py
@@ -88,7 +88,12 @@
     conditioned = jax.nn.silu(jnp.stack([cond_latent, cond_context])).astype(jnp.bfloat16)
     partial_mod = jnp.dot(conditioned, mod_weight, preferred_element_type=jnp.float32)
     summed = lax.psum(partial_mod, "sp")
-    modulation = lax.all_gather(summed, "tp", axis=1, tiled=True)
+    ring = [summed]
+    for hop in range(7):
+        ring.append(lax.ppermute(ring[-1], "tp", [(dev, (dev + 1) % 8) for dev in range(8)]))
+    modulation = jnp.roll(
+        jnp.concatenate(ring[::-1], axis=1), (lax.axis_index("tp") + 1) * ring[0].shape[1], axis=1
+    )
     shift_context = modulation[1, :width]
     scale_context = modulation[1, width : 2 * width]
     gate_latent = modulation[0, 2 * width :]

time: 154 us -> 161 us (1.045)
  waiting for transfers between devices: 2.24 us -> 35.1 us
  blocking collectives: 130 us -> 102 us
    ppermute x0 -> x7, waiting for transfers between devices: none -> 31.2 us  [shards(): lax.ppermute(ring[-1], 'tp', [(dev, (dev + 1) % 8) for dev in range(8)])]
    all_gather x1 -> x0, blocking collectives: 28.2 us -> none  [shards(): modulation = lax.all_gather(summed, 'tp', axis=1, tiled=True)]
    all_gather x1, blocking collectives: 33 us -> 37.8 us  [shards(): piece = lax.all_gather(own_rows, 'tp', axis=0, tiled=True)]
    unnamed x1, blocking collectives: 48.5 us -> 44.5 us
    ppermute x0 -> x7, starting transfers between devices: none -> 2.18 us  [shards(): lax.ppermute(ring[-1], 'tp', [(dev, (dev + 1) % 8) for dev in range(8)])]
    unnamed x1, waiting for transfers between devices: 2.24 us -> 3.95 us
  transfers between devices with their start and end apart: 1 -> 8, of which waited for: 1 -> 8; matrix products, arithmetic and copies ran while one was open for 0% -> 2% of each run, Pallas kernels for 0% -> 0%
where the time goes in v1:
time: 161 us; the launch traced here: 160 us
  blocking collectives  102 us (63%)
  waiting for transfers between devices  35.1 us (22%)
  matrix products  7.09 us (4%)
  starting transfers between devices  5.81 us (4%)
  other arithmetic  4.83 us (3%)
  local copies, waits for them, and re-layouts  3.3 us (2%)
  between operations  1.67 us (1%)
    unnamed x1, blocking collectives  44.5 us
    all_gather x1, blocking collectives, shards(): piece = lax.all_gather(own_rows, 'tp', axis=0, tiled=True)  37.8 us
    ppermute x7, waiting for transfers between devices, shards(): lax.ppermute(ring[-1], 'tp', [(dev, (dev + 1) % 8) for dev in range(8)])  31.2 us
    psum x1, blocking collectives, shards(): summed = lax.psum(partial_mod, 'sp')  7.04 us
    all_gather x1, blocking collectives, shards(): lax.all_gather(joined_values, 'sp', axis=0, tiled=True)  6.83 us
    all_gather x1, blocking collectives, shards(): lax.all_gather(joined_keys, 'sp', axis=0, tiled=True)  6.28 us
    unnamed x1, waiting for transfers between devices  3.95 us
    unnamed x1, starting transfers between devices  3.62 us
  transfers between devices with their start and end apart: 8, of which 8 were waited for; matrix products, arithmetic and copies ran while one was open for 2% of the time, Pallas kernels for 0%

profile of v1, /device:TPU:8, one launch (start us, length us, event | category | flops | bytes accessed | tf_op | source)
XLA Modules:
  0.0 160.2 jit_solution(11692758033670076608)
XLA Ops:
  0.0 1.1 copy-done
  1.1 0.9 fusion.37
  2.0 7.0 %psum.7 = f32[2,768]{1,0:T(2,128)S(1)} all-reduce(f32[2,768]{1,0:T(2,128)S(1)} %fusion.37), channel_id=1, replica_groups=mesh['sp'=4,'tp'=8] {'sp'}, use_global_device_ids=true, to_apply=%region_0.1 | all-reduce | flops 1536 | bytes 12288 | tf_op jit(solution)/shard_map/psum | solution.py:90
  9.1 1.5 collective-permute-start
  10.7 3.0 %collective-permute-done = f32[2,768]{1,0:T(2,128)S(1)} collective-permute-done((f32[2,768]{1,0:T(2,128)S(1)}, f32[2,768]{1,0:T(2,128)S(1)}, u32[]{:S(2)}, u32[]{:S(2)}) %collective-permute-start) | collective-permute-done | bytes 6176 | tf_op jit(solution)/shard_map/ppermute | solution.py:93
  14.4 3.8 %collective-permute-done.1 = f32[2,768]{1,0:T(2,128)S(1)} collective-permute-done((f32[2,768]{1,0:T(2,128)S(1)}, f32[2,768]{1,0:T(2,128)S(1)}, u32[]{:S(2)}, u32[]{:S(2)}) %collective-permute-start.1) | collective-permute-done | bytes 6176 | tf_op jit(solution)/shard_map/ppermute | solution.py:93
  18.2 1.4 fusion.6
  19.6 3.2 %collective-permute-done.2 = f32[2,768]{1,0:T(2,128)S(1)} collective-permute-done((f32[2,768]{1,0:T(2,128)S(1)}, f32[2,768]{1,0:T(2,128)S(1)}, u32[]{:S(2)}, u32[]{:S(2)}) %collective-permute-start.2) | collective-permute-done | bytes 6176 | tf_op jit(solution)/shard_map/ppermute | solution.py:93
  22.7 4.5 %collective-permute-done.3 = f32[2,768]{1,0:T(2,128)S(1)} collective-permute-done((f32[2,768]{1,0:T(2,128)S(1)}, f32[2,768]{1,0:T(2,128)S(1)}, u32[]{:S(2)}, u32[]{:S(2)}) %collective-permute-start.3) | collective-permute-done | bytes 6176 | tf_op jit(solution)/shard_map/ppermute | solution.py:93
  27.3 1.0 fusion.14
  28.3 4.9 %collective-permute-done.4 = f32[2,768]{1,0:T(2,128)S(1)} collective-permute-done((f32[2,768]{1,0:T(2,128)S(1)}, f32[2,768]{1,0:T(2,128)S(1)}, u32[]{:S(2)}, u32[]{:S(2)}) %collective-permute-start.4) | collective-permute-done | bytes 6176 | tf_op jit(solution)/shard_map/ppermute | solution.py:93
  33.3 6.3 %collective-permute-done.5 = f32[2,768]{1,0:T(2,128)S(1)} collective-permute-done((f32[2,768]{1,0:T(2,128)S(1)}, f32[2,768]{1,0:T(2,128)S(1)}, u32[]{:S(2)}, u32[]{:S(2)}) %collective-permute-start.5) | collective-permute-done | bytes 6176 | tf_op jit(solution)/shard_map/ppermute | solution.py:93
  40.5 5.4 %collective-permute-done.6 = f32[2,768]{1,0:T(2,128)S(1)} collective-permute-done((f32[2,768]{1,0:T(2,128)S(1)}, f32[2,768]{1,0:T(2,128)S(1)}, u32[]{:S(2)}, u32[]{:S(2)}) %collective-permute-start.6) | collective-permute-done | bytes 6176 | tf_op jit(solution)/shard_map/ppermute | solution.py:93
  47.3 37.8 %all-gather = bf16[8,30,2048]{2,1,0:T(8,128)(2,1)S(1)} all-gather(bf16[1,30,2048]{2,1,0:T(8,128)(2,1)S(1)} %fusion.19), channel_id=1, replica_groups=mesh['sp'=4,'tp'=8] {'tp'}, dimensions={0}, use_global_device_ids=true | all-gather | bytes 1105920 | tf_op jit(solution)/shard_map/all_gather | solution.py:103
  85.4 1.5 convolution_convert_fusion
  86.9 1.4 fusion.48
  89.4 6.3 %all_gather.10 = bf16[1728,128]{1,0:T(8,128)(2,1)S(1)} all-gather(bf16[432,128]{1,0:T(8,128)(2,1)S(1)} %pad_maximum_fusion), channel_id=1, replica_groups=mesh['sp'=4,'tp'=8] {'sp'}, dimensions={0}, use_global_device_ids=true | all-gather | bytes 552960 | tf_op jit(solution)/shard_map/all_gather | solution.py:131
  95.9 6.8 %all_gather.11 = bf16[1728,128]{1,0:T(8,128)(2,1)S(1)} all-gather(bf16[432,128]{1,0:T(8,128)(2,1)S(1)} %pad_maximum_fusion.1), channel_id=1, replica_groups=mesh['sp'=4,'tp'=8] {'sp'}, dimensions={0}, use_global_device_ids=true | all-gather | bytes 552960 | tf_op jit(solution)/shard_map/all_gather | solution.py:132
  102.8 0.7 fusion.46
  104.1 0.7 fusion.10
  105.7 44.5 %fusion = f32[32,2048]{1,0:T(8,128)S(1)} fusion(f32[240,2048]{1,0:T(8,128)S(1)} %fusion.28), kind=kCustom, calls=%all-reduce-scatter | all-reduce-scatter fusion | flops 524289 | bytes 2228736
  150.2 3.6 %collective-permute-start.7 = (f32[14,2048]{1,0:T(8,128)S(1)}, f32[14,2048]{1,0:T(8,128)S(1)}, u32[]{:S(2)}, u32[]{:S(2)}) collective-permute-start(f32[14,2048]{1,0:T(8,128)S(1)} %slice.92), channel_id=1, source_target_pairs={{0,1},{1,2},{2,3},{3,4},{4,5},{5,6},{6,7},{8,9},{9,10},{10,11},{11... | collective-permute-start | bytes 344072
  155.1 4.0 %collective-permute-done.7 = f32[14,2048]{1,0:T(8,128)S(1)} collective-permute-done((f32[14,2048]{1,0:T(8,128)S(1)}, f32[14,2048]{1,0:T(8,128)S(1)}, u32[]{:S(2)}, u32[]{:S(2)}) %collective-permute-start.7) | collective-permute-done | bytes 114720
  159.4 0.8 fusion.18
  (73 shorter events, 6.3 us)
Async XLA Ops:
  0.0 1.1 copy-start
  0.0 46.2 %copy-start.2 = (bf16[192,2048]{1,0:T(8,128)(2,1)S(1)}, bf16[192,2048]{1,0:T(8,128)(2,1)}, u32[]{:S(2)}) copy-start(bf16[192,2048]{1,0:T(8,128)(2,1)} %param.11) | copy-start | bytes 2359300
  0.0 46.3 %copy-start.3 = (bf16[2048,128]{1,0:T(8,128)(2,1)S(1)}, bf16[2048,128]{1,0:T(8,128)(2,1)}, u32[]{:S(2)}) copy-start(bf16[2048,128]{1,0:T(8,128)(2,1)} %param.17) | copy-start | bytes 1572868
  9.1 4.6 %collective-permute-start = (f32[2,768]{1,0:T(2,128)S(1)}, f32[2,768]{1,0:T(2,128)S(1)}, u32[]{:S(2)}, u32[]{:S(2)}) collective-permute-start(f32[2,768]{1,0:T(2,128)S(1)} %psum.7), channel_id=1, source_target_pairs={{0,1},{1,2},{2,3},{3,4},{4,5},{5,6},{6,7},{7,0},{8,9},{9,10},{10,1... | collective-permute-start | bytes 18440 | tf_op jit(solution)/shard_map/ppermute | solution.py:93
  13.7 4.5 %collective-permute-start.1 = (f32[2,768]{1,0:T(2,128)S(1)}, f32[2,768]{1,0:T(2,128)S(1)}, u32[]{:S(2)}, u32[]{:S(2)}) collective-permute-start(f32[2,768]{1,0:T(2,128)S(1)} %collective-permute-done), channel_id=1, source_target_pairs={{0,1},{1,2},{2,3},{3,4},{4,5},{5,6},{6,7},{7,0},{8,9},{9,10},{10,1... | collective-permute-start | bytes 18440 | tf_op jit(solution)/shard_map/ppermute | solution.py:93
  14.4 32.4 %copy-start.4 = (bf16[2048,128]{1,0:T(8,128)(2,1)S(1)}, bf16[2048,128]{1,0:T(8,128)(2,1)}, u32[]{:S(2)}) copy-start(bf16[2048,128]{1,0:T(8,128)(2,1)} %param.16) | copy-start | bytes 1572868
  18.2 4.5 %collective-permute-start.2 = (f32[2,768]{1,0:T(2,128)S(1)}, f32[2,768]{1,0:T(2,128)S(1)}, u32[]{:S(2)}, u32[]{:S(2)}) collective-permute-start(f32[2,768]{1,0:T(2,128)S(1)} %collective-permute-done.1), channel_id=1, source_target_pairs={{0,1},{1,2},{2,3},{3,4},{4,5},{5,6},{6,7},{7,0},{8,9},{9,10},{10,1... | collective-permute-start | bytes 18440 | tf_op jit(solution)/shard_map/ppermute | solution.py:93
  22.7 4.5 %collective-permute-start.3 = (f32[2,768]{1,0:T(2,128)S(1)}, f32[2,768]{1,0:T(2,128)S(1)}, u32[]{:S(2)}, u32[]{:S(2)}) collective-permute-start(f32[2,768]{1,0:T(2,128)S(1)} %collective-permute-done.2), channel_id=1, source_target_pairs={{0,1},{1,2},{2,3},{3,4},{4,5},{5,6},{6,7},{7,0},{8,9},{9,10},{10,1... | collective-permute-start | bytes 18440 | tf_op jit(solution)/shard_map/ppermute | solution.py:93
  27.3 6.0 %collective-permute-start.4 = (f32[2,768]{1,0:T(2,128)S(1)}, f32[2,768]{1,0:T(2,128)S(1)}, u32[]{:S(2)}, u32[]{:S(2)}) collective-permute-start(f32[2,768]{1,0:T(2,128)S(1)} %collective-permute-done.3), channel_id=1, source_target_pairs={{0,1},{1,2},{2,3},{3,4},{4,5},{5,6},{6,7},{7,0},{8,9},{9,10},{10,1... | collective-permute-start | bytes 18440 | tf_op jit(solution)/shard_map/ppermute | solution.py:93
  33.3 6.3 %collective-permute-start.5 = (f32[2,768]{1,0:T(2,128)S(1)}, f32[2,768]{1,0:T(2,128)S(1)}, u32[]{:S(2)}, u32[]{:S(2)}) collective-permute-start(f32[2,768]{1,0:T(2,128)S(1)} %collective-permute-done.4), channel_id=1, source_target_pairs={{0,1},{1,2},{2,3},{3,4},{4,5},{5,6},{6,7},{7,0},{8,9},{9,10},{10,1... | collective-permute-start | bytes 18440 | tf_op jit(solution)/shard_map/ppermute | solution.py:93
  39.6 6.3 %collective-permute-start.6 = (f32[2,768]{1,0:T(2,128)S(1)}, f32[2,768]{1,0:T(2,128)S(1)}, u32[]{:S(2)}, u32[]{:S(2)}) collective-permute-start(f32[2,768]{1,0:T(2,128)S(1)} %collective-permute-done.5), channel_id=1, source_target_pairs={{0,1},{1,2},{2,3},{3,4},{4,5},{5,6},{6,7},{7,0},{8,9},{9,10},{10,1... | collective-permute-start | bytes 18440 | tf_op jit(solution)/shard_map/ppermute | solution.py:93
  46.3 0.9 copy-start.1
  85.4 3.0 %copy-start.5 = (bf16[2048,128]{1,0:T(8,128)(2,1)S(1)}, bf16[2048,128]{1,0:T(8,128)(2,1)}, u32[]{:S(2)}) copy-start(bf16[2048,128]{1,0:T(8,128)(2,1)} %param.15) | copy-start | bytes 1572868
  104.1 1.0 copy-start.6
  105.2 48.6 %copy-start.7 = (u32[32]{0:T(128)S(1)}, u32[32]{0:T(128)}, u32[]{:S(2)}) copy-start(u32[32]{0:T(128)} %constant.94) | copy-start | bytes 388
  150.2 8.8 %collective-permute-start.7 = (f32[14,2048]{1,0:T(8,128)S(1)}, f32[14,2048]{1,0:T(8,128)S(1)}, u32[]{:S(2)}, u32[]{:S(2)}) collective-permute-start(f32[14,2048]{1,0:T(8,128)S(1)} %slice.92), channel_id=1, source_target_pairs={{0,1},{1,2},{2,3},{3,4},{4,5},{5,6},{6,7},{8,9},{9,10},{10,11},{11... | collective-permute-start | bytes 344072
